TPU v7x, 128 devices: a whole 4x4x4 slice. The times are simulated.
128 devices in a mesh: ep: 64 (over z, y, x), tp: 2 (over core).
Axes of the slice: x: 4, y: 4, z: 4, core: 2. Of those that a mesh axis runs over, the one named last changes fastest.
Arguments:
- inputs: bfloat16 [1024, 2048], P('ep'), may hold values from -6 to 6
- positions: int32 [1024], P('ep'), may hold values from 1024 to 8191
- ret_state: float32 [1024, 12, 128, 128], P('ep', 'tp'), may hold values from -4 to 4
- norm_mix: bfloat16 [2048], replicated, may hold values from 0.099609375 to 1.8984375
- w_query: bfloat16 [2048, 1536], P('ep', 'tp'), may hold values from -0.375 to 0.375
- w_key: bfloat16 [2048, 1536], P('ep', 'tp'), may hold values from -0.375 to 0.375
- w_value: bfloat16 [2048, 1536], P('ep', 'tp'), may hold values from -0.375 to 0.375
- w_gate_in: bfloat16 [2048, 1536], P('ep', 'tp'), may hold values from -0.375 to 0.375
- head_gain: bfloat16 [1536], P('tp'), may hold values from 0.099609375 to 1.8984375
- w_out: bfloat16 [1536, 2048], P('tp', 'ep'), may hold values from -0.15625 to 0.15625
- norm_ffn: bfloat16 [2048], replicated, may hold values from 0.099609375 to 1.8984375
- route_ids: int32 [1024, 4], P('ep'), may hold values from 0 to 63, all different within a row; in each aligned block of 16 rows (0 to 15, 16 to 31, ...) at most 2 rows name the same one
- route_weight: bfloat16 [1024, 4], P('ep'), may hold values from 0.19921875 to 1
- exp_gate: bfloat16 [64, 2048, 1024], P('ep', None, 'tp'), may hold values from -0.125 to 0.125
- exp_up: bfloat16 [64, 2048, 1024], P('ep', None, 'tp'), may hold values from -0.125 to 0.125
- exp_down: bfloat16 [64, 1024, 2048], P('ep', 'tp'), may hold values from -0.1875 to 0.1875
- dense_gate: bfloat16 [2048, 4096], P(None, ('ep', 'tp')), may hold values from -0.125 to 0.125
- dense_up: bfloat16 [2048, 4096], P(None, ('ep', 'tp')), may hold values from -0.125 to 0.125
- dense_down: bfloat16 [4096, 2048], P(('ep', 'tp')), may hold values from -0.375 to 0.375
- branch_gate: bfloat16 [2048], replicated, may hold values from -0.125 to 0.125
Outputs:
- layer_out: bfloat16 [1024, 2048], P('ep')
- new_state: float32 [1024, 12, 128, 128], P('ep', 'tp')
Inputs may be any that keep to these rules, and one draw needn't show every extreme that they name: `route_ids`: each row names 4 different experts. Among the rows of one index of ep no expert is named more than 2 times, a bound that some block reaches.
All inputs are finite; a program needn't handle non-finite values.
Results may differ from a plain program's by a relative error of at most 0.015.
Values may be sent and summed in bfloat16 or wider, within the bound.
No kernel may reach another device: no remote copies, remote signals or barrier semaphores. Data moves between devices by JAX's collectives and lax.ppermute only.
A program may use at most 128 MiB of HBM per device.

v0:
```python
import jax
import jax.numpy as jnp
from jax import lax
from jax.sharding import PartitionSpec as P

D = 2048
HEADS = 12
EPS = 1e-06


def in_one_piece(arrays, axis, dim, along):
    both = jnp.concatenate(arrays, axis=along)
    out, at, done = (lax.all_gather(both, axis, axis=dim, tiled=True), 0, [])
    for a in arrays:
        done.append(lax.slice_in_dim(out, at, at + a.shape[along], axis=along))
        at += a.shape[along]
    return tuple(done)


def sent_to_all(array, axis):
    copies = jnp.broadcast_to(array, (lax.axis_size(axis), *array.shape))
    return lax.all_to_all(copies, axis, split_axis=0, concat_axis=0, tiled=True)


def over_copies(array, axis):
    everything = sent_to_all(array, axis)
    return jnp.sum(everything.astype(jnp.float32), axis=0)


def split_up(array, dim, size):
    before, after = (array.shape[:dim], array.shape[dim + 1 :])
    return jnp.moveaxis(array.reshape(*before, size, -1, *after), dim, 0)


def summed_on_arrival(array, axis, dim):
    size = lax.axis_size(axis)
    tiles = lax.all_to_all(split_up(array, dim, size), axis, 0, 0, tiled=True)
    return jnp.sum(tiles.astype(jnp.float32), axis=0)


def rms_scale(values, scales):
    widened = values.astype(jnp.float32)
    scaled = widened * lax.rsqrt(jnp.mean(widened * widened, axis=-1, keepdims=True) + EPS)
    return (scaled * scales.astype(jnp.float32)).astype(jnp.bfloat16)


def rotary_angles(positions, head_dim):
    halfway = head_dim // 2
    frequency = 10000.0 ** (-jnp.arange(halfway, dtype=jnp.float32) * 2.0 / head_dim)
    return positions.astype(jnp.float32)[:, None] * frequency[None, :]


def rotate_heads(values, angles):
    halfway = values.shape[-1] // 2
    cosine = jnp.cos(angles)[:, None, :]
    sine_of = jnp.sin(angles)[:, None, :]
    leading = values[..., :halfway]
    trailing = values[..., halfway:]
    return jnp.concatenate(
        [leading * cosine - trailing * sine_of, trailing * cosine + leading * sine_of], axis=-1
    )


def log_decay(head_count):
    spread = jnp.arange(head_count, dtype=jnp.float32) * (5.0 / max(head_count - 1, 1))
    return jnp.log1p(-(2.0 ** (-5.0 - spread)))


def retain(queries, keys_in, values_in, gate_pre, old_state, positions, scales, log_gamma):
    row_count, head_count, head_dim = (old_state.shape[0], old_state.shape[1], old_state.shape[2])
    angles = rotary_angles(positions, head_dim)
    rot_query = rotate_heads(
        queries.astype(jnp.float32).reshape(row_count, head_count, head_dim), angles
    )
    rot_key = rotate_heads(
        keys_in.astype(jnp.float32).reshape(row_count, head_count, head_dim), angles
    ) * head_dim ** (-0.5)
    value_heads = values_in.astype(jnp.float32).reshape(row_count, head_count, head_dim)
    new_state = (
        jnp.exp(log_gamma)[None, :, None, None] * old_state
        + rot_key[:, :, :, None] * value_heads[:, :, None, :]
    )
    readout = jnp.einsum("shd,shdv->shv", rot_query, new_state, precision=lax.Precision.HIGHEST)
    centred = readout - jnp.mean(readout, axis=-1, keepdims=True)
    normed = centred * lax.rsqrt(jnp.mean(centred * centred, axis=-1, keepdims=True) + EPS)
    normed = normed * scales.astype(jnp.float32).reshape(head_count, head_dim)
    gated_out = normed.reshape(row_count, head_count * head_dim) * jax.nn.silu(
        gate_pre.astype(jnp.float32)
    )
    return (gated_out.astype(jnp.bfloat16), new_state)


def slot_of(route_ids, expert_count, capacity):
    flat_ids = route_ids.reshape(-1)
    onehot = (flat_ids[:, None] == jnp.arange(expert_count, dtype=jnp.int32)[None, :]).astype(
        jnp.int32
    )
    ranking = jnp.sum((jnp.cumsum(onehot, axis=0) - 1) * onehot, axis=1)
    return flat_ids * capacity + ranking


def on_device(
    inputs,
    positions,
    ret_state,
    norm_mix,
    w_query,
    w_key,
    w_value,
    w_gate_in,
    head_gain,
    w_out,
    norm_ffn,
    route_ids,
    route_weight,
    exp_gate,
    exp_up,
    exp_down,
    dense_gate,
    dense_up,
    dense_down,
    branch_gate,
):
    seq_count = inputs.shape[0]
    top_count = route_ids.shape[1]
    ep_size = lax.axis_size("ep")
    local_experts = exp_gate.shape[0]
    expert_count = ep_size * local_experts
    capacity = max(2, 2 * seq_count * top_count // expert_count)
    normed = rms_scale(inputs, norm_mix)
    segments = in_one_piece((w_query, w_key, w_value, w_gate_in), "ep", 0, 1)
    totals = tuple(
        (
            jnp.dot(normed, weight_rows, preferred_element_type=jnp.float32)
            for weight_rows in segments
        )
    )
    queries, keys_new, values_new, gate_pre = [member.astype(jnp.bfloat16) for member in totals]
    local_heads = ret_state.shape[1]
    log_gamma = lax.dynamic_slice_in_dim(
        log_decay(HEADS), lax.axis_index("tp") * local_heads, local_heads
    )
    retained, new_state = retain(
        queries, keys_new, values_new, gate_pre, ret_state, positions, head_gain, log_gamma
    )
    partial_rows = jnp.dot(
        retained,
        lax.all_gather(w_out, "ep", axis=1, tiled=True),
        preferred_element_type=jnp.float32,
    )
    rounded = lax.optimization_barrier(partial_rows.astype(jnp.bfloat16)).astype(jnp.float32)
    mixer_out = (
        over_copies(rounded.astype(jnp.bfloat16), "tp").astype(jnp.float32).astype(jnp.bfloat16)
    )
    residual_sum = (inputs.astype(jnp.float32) + mixer_out.astype(jnp.float32)).astype(jnp.bfloat16)
    normed_ffn = rms_scale(residual_sum, norm_ffn)
    slot_index = slot_of(route_ids, expert_count, capacity)
    slot_total = expert_count * capacity
    placing = (jnp.arange(slot_total, dtype=jnp.int32)[:, None] == slot_index[None, :]).astype(
        jnp.float32
    )
    by_token = jnp.sum(placing.reshape(slot_total, seq_count, top_count), axis=2)
    outgoing = (
        jnp.dot(by_token.astype(jnp.bfloat16), normed_ffn, preferred_element_type=jnp.float32)
        .astype(jnp.bfloat16)
        .reshape(expert_count, capacity, D)
    )
    received = lax.all_to_all(outgoing, "ep", split_axis=0, concat_axis=0, tiled=True)
    slot_count = received.shape[1]
    grouped = received.reshape(ep_size, local_experts, slot_count, D)
    gate_part = jnp.einsum("sjnd,jdf->sjnf", grouped, exp_gate, preferred_element_type=jnp.float32)
    up_part = jnp.einsum("sjnd,jdf->sjnf", grouped, exp_up, preferred_element_type=jnp.float32)
    hidden = (jax.nn.silu(gate_part) * up_part).astype(jnp.bfloat16)
    partial_out = jnp.einsum(
        "sjnf,jfd->sjnd", hidden, exp_down, preferred_element_type=jnp.float32
    ).reshape(received.shape[0], slot_count, D)
    returned = lax.all_to_all(
        partial_out.astype(jnp.bfloat16), "ep", split_axis=0, concat_axis=0, tiled=True
    ).astype(partial_out.dtype)
    widened = route_weight.astype(jnp.float32)
    share_flat = (widened / jnp.sum(widened, axis=-1, keepdims=True)).reshape(-1)
    weighting = jnp.sum(
        (placing * share_flat[None, :]).reshape(slot_total, seq_count, top_count), axis=2
    )
    expert_part = jnp.einsum(
        "rt,rd->td", weighting, returned.reshape(slot_total, D), precision=lax.Precision.HIGHEST
    )
    segment = lax.all_gather(normed_ffn, "ep", axis=0, tiled=True)
    gate_part = jnp.dot(segment, dense_gate, preferred_element_type=jnp.float32)
    up_part = jnp.dot(segment, dense_up, preferred_element_type=jnp.float32)
    hidden = (jax.nn.silu(gate_part) * up_part).astype(jnp.bfloat16)
    opening = jax.nn.sigmoid(
        jnp.dot(segment, branch_gate[:, None], preferred_element_type=jnp.float32)
    )
    branch_term = jnp.dot(hidden, dense_down, preferred_element_type=jnp.float32) * opening
    summed_branch = summed_on_arrival(branch_term.astype(jnp.bfloat16), "ep", 0)
    summed_branch = summed_branch + expert_part
    width_total = over_copies(summed_branch.astype(jnp.bfloat16), "tp").astype(jnp.float32)
    layer_out = (residual_sum.astype(jnp.float32) + width_total).astype(jnp.bfloat16)
    return (layer_out, new_state)


def solution(mesh):
    in_specs = (
        P("ep", None),
        P("ep"),
        P("ep", "tp", None, None),
        P(),
        P("ep", "tp"),
        P("ep", "tp"),
        P("ep", "tp"),
        P("ep", "tp"),
        P("tp"),
        P("tp", "ep"),
        P(),
        P("ep", None),
        P("ep", None),
        P("ep", None, "tp"),
        P("ep", None, "tp"),
        P("ep", "tp", None),
        P(None, ("ep", "tp")),
        P(None, ("ep", "tp")),
        P(("ep", "tp"), None),
        P(),
    )
    out_specs = (P("ep", None), P("ep", "tp", None, None))
    return jax.shard_map(
        on_device, mesh=mesh, in_specs=in_specs, out_specs=out_specs, check_vma=False
    )
```

profile of v0, /device:TPU:1, one launch (start us, length us, event | category | flops | bytes accessed | tf_op | source)
XLA Modules:
  0.0 340.6 jit_solution(12423903585357650774)
XLA Ops:
  7.2 1.7 pad_maximum_fusion
  9.0 0.7 all-gather.6.cloned.1.call-update
  9.8 0.7 convert_element_type.100
  10.5 0.7 convert_element_type.103
  11.1 0.7 convert_element_type.113
  11.9 1.0 fusion.64
  12.9 0.7 bitcast_convert_fusion
  13.6 0.1 multiply_cosine_fusion
  13.7 91.6 %all-gather.4.cloned.1.call-done = bf16[2048,3072]{1,0:T(8,128)(2,1)} async-done(((bf16[32,3072]{1,0:T(8,128)(2,1)}), bf16[2048,3072]{1,0:T(8,128)(2,1)}) %all-gather.4.cloned.1.call-update) | async-done | bytes 12582928 | tf_op jit(solution)/shard_map/all_gather | solution.py:13
  105.3 2.5 fusion.33
  107.8 2.5 fusion.39
  110.4 2.4 fusion.45
  112.8 0.1 multiply_subtract_fusion.1
  112.9 0.1 maximum_multiply_fusion
  113.1 4.5 %multiply_add_fusion = f32[16,6,128,128]{3,2,1,0:T(8,128)S(1)} fusion(f32[16,6,128,128]{3,2,1,0:T(8,128)} %param.22, f32[16,6,128]{2,1,0:T(8,128)S(1)} %reshape.207, f32[16,6,128]{2,1,0:T(8,128)S(1)} %maximum_multiply_fusion, f32[6]{0:T(128)S(1)} %dynamic-slice_exponential_fusion), kind=kLoop, calls=%fused_computation.2 | loop fusion | flops 4718592 | bytes 12681240 | tf_op jit(solution)/shard_map/add | solution.py:80
  117.6 2.7 copy-done.2
  120.3 5.5 %fusion.84 = f32[16,6,1,128]{3,2,1,0:T(1,128)S(1)} fusion(f32[16,6,128,128]{3,2,1,0:T(8,128)S(1)} %multiply_add_fusion, f32[16,6,128,1]{2,1,0,3:T(8,128)S(1)} %maximum_bitcast_fusion), kind=kOutput, calls=%fused_computation.80 | convolution fusion | flops 18874368 | bytes 6389760 | tf_op jit(solution)/shard_map/shd,shdv->shv/dot_general | solution.py:83
  125.8 0.1 bitcast_reduce_fusion
  125.9 0.2 fusion.80
  126.0 0.1 fusion.81
  126.2 47.2 %all-gather.6.cloned.1.call-done = bf16[768,2048]{0,1:T(8,128)(2,1)} async-done(((bf16[768,32]{0,1:T(8,128)(2,1)}), bf16[768,2048]{0,1:T(8,128)(2,1)}) %all-gather.6.cloned.1.call-update) | async-done | bytes 3145744 | tf_op jit(solution)/shard_map/all_gather | solution.py:148
  173.4 4.5 %convolution_convert_fusion.2 = bf16[16,2048]{1,0:T(8,128)(2,1)S(1)} fusion(bf16[768,2048]{0,1:T(8,128)(2,1)} %all-gather.6.cloned.1.call-done, f32[2,8,6,128]{3,2,1,0:T(8,128)S(1)} %bitcast.87, bf16[2048,3072]{1,0:T(8,128)(2,1)} %all-gather.4.cloned.1.call-done, bf16[16,2048]{1,0:T(8,128)(2,1)S(1)} %copy-done.3, f32[2048]{0:T(1024)S(1)} %convert_element_type.100, ...), kind=kOutput, calls=%fused_computation.15 | convolution fusion | flops 100925440 | bytes 6479936 | tf_op jit(solution)/shard_map/dot_general | solution.py:146
  177.9 5.7 %all_to_all.25 = bf16[2,16,2048]{2,1,0:T(8,128)(2,1)S(1)} all-to-all(bf16[2,16,2048]{2,1,0:T(8,128)(2,1)S(1)} %broadcast_in_dim.4), channel_id=1, replica_groups=mesh['ep'=64,'tp'=2] {'tp'}, dimensions={0} | all-to-all | bytes 262144 | tf_op jit(solution)/shard_map/all_to_all | solution.py:22
  183.6 0.1 fusion.68
  183.8 0.7 fusion.70
  184.6 0.1 eq.31
  184.8 0.1 reduce_window_sum.11
  184.9 0.2 select_reduce_fusion.1
  185.1 0.1 copy.44
  185.4 1.2 convolution_convert_fusion.1
  186.5 1.1 reshape.197
  187.7 6.1 %all-to-all-start.2 = ((bf16[64,2,2048]{2,1,0:T(2,128)(2,1)}), bf16[64,2,2048]{2,1,0:T(2,128)(2,1)S(1)}, u32[]{:S(2)}, u32[]{:S(2)}) async-start(bf16[64,2,2048]{2,1,0:T(2,128)(2,1)} %reshape.197), calls=%async_computation.2 | async-start | bytes 1048576 | tf_op jit(solution)/shard_map/all_to_all | solution.py:168
  193.8 12.9 %all-to-all-done.2 = bf16[64,2,2048]{2,1,0:T(2,128)(2,1)S(1)} async-done(((bf16[64,2,2048]{2,1,0:T(2,128)(2,1)}), bf16[64,2,2048]{2,1,0:T(2,128)(2,1)S(1)}, u32[]{:S(2)}, u32[]{:S(2)}) %all-to-all-start.2) | async-done | bytes 524320 | tf_op jit(solution)/shard_map/all_to_all | solution.py:168
  206.7 2.0 fusion.14
  208.8 2.4 convolution_convert_fusion
  211.2 1.4 copy.47
  212.6 4.8 %all-to-all-start.3 = ((bf16[64,2,2048]{2,1,0:T(2,128)(2,1)}), bf16[64,2,2048]{2,1,0:T(2,128)(2,1)S(1)}, u32[]{:S(2)}, u32[]{:S(2)}) async-start(bf16[64,2,2048]{2,1,0:T(2,128)(2,1)} %copy.47), calls=%async_computation.3 | async-start | bytes 1048576 | tf_op jit(solution)/shard_map/all_to_all | solution.py:177
  217.5 36.3 %all-gather.8.cloned.1.call-done = bf16[1024,2048]{1,0:T(8,128)(2,1)} async-done(((bf16[16,2048]{1,0:T(8,128)(2,1)}), bf16[1024,2048]{1,0:T(8,128)(2,1)}) %all-gather.8.cloned.1.call-update) | async-done | bytes 4194320 | tf_op jit(solution)/shard_map/all_gather | solution.py:188
  253.8 3.7 %fusion.101 = f32[1024,32]{0,1:T(8,128)S(1)} fusion(bf16[1024,2048]{1,0:T(8,128)(2,1)} %all-gather.8.cloned.1.call-done, bf16[2048,32]{0,1:T(8,128)(2,1)} %param.36), kind=kOutput, calls=%fused_computation.107 | convolution fusion | flops 134217728 | bytes 4456448 | tf_op jit(solution)/shard_map/dot_general | solution.py:189
  257.5 1.2 fusion.102
  258.7 6.7 %multiply_convert_fusion = bf16[1024,2048]{1,0:T(8,128)(2,1)} fusion(bf16[32,2048]{1,0:T(8,128)(2,1)S(1)} %copy-done.4, f32[1024]{0:T(1024)S(1)} %add_divide_fusion, bf16[1024,2048]{1,0:T(8,128)(2,1)} %all-gather.8.cloned.1.call-done, bf16[2048,32]{0,1:T(8,128)(2,1)S(1)} %copy-done.5, f32[1024,32]{0,1:T(8,128)S(1)} %fusion.101), kind=kOutput, calls=%fused_computation.1 | convolution fusion | flops 272826368 | bytes 8785920 | tf_op jit(solution)/shard_map/dot_general | solution.py:195
  265.4 6.8 %all-to-all-start.1 = ((bf16[64,16,2048]{2,1,0:T(8,128)(2,1)}), bf16[64,16,2048]{2,1,0:T(8,128)(2,1)}, u32[]{:S(2)}, u32[]{:S(2)}) async-start(bf16[64,16,2048]{2,1,0:T(8,128)(2,1)} %bitcast.86), calls=%async_computation.1 | async-start | bytes 8388608 | tf_op jit(solution)/shard_map/all_to_all | solution.py:37
  272.2 0.2 reshape.202
  272.4 50.4 %all-to-all-done.1 = bf16[64,16,2048]{2,1,0:T(8,128)(2,1)} async-done(((bf16[64,16,2048]{2,1,0:T(8,128)(2,1)}), bf16[64,16,2048]{2,1,0:T(8,128)(2,1)}, u32[]{:S(2)}, u32[]{:S(2)}) %all-to-all-start.1) | async-done | bytes 4194336 | tf_op jit(solution)/shard_map/all_to_all | solution.py:37
  322.8 2.9 convert_reduce_fusion
  325.6 0.3 fusion.8
  326.0 7.5 %all_to_all.26 = bf16[2,16,2048]{2,1,0:T(8,128)(2,1)S(1)} all-to-all(bf16[2,16,2048]{2,1,0:T(8,128)(2,1)S(1)} %broadcast_in_dim.5), channel_id=1, replica_groups=mesh['ep'=64,'tp'=2] {'tp'}, dimensions={0} | all-to-all | bytes 262144 | tf_op jit(solution)/shard_map/all_to_all | solution.py:22
  333.4 0.7 fusion.71
  (47 shorter events, 0.9 us)
Async XLA Ops:
  7.2 201.6 %copy-start = (bf16[1,512,2048]{2,1,0:T(8,128)(2,1)S(1)}, bf16[1,512,2048]{2,1,0:T(8,128)(2,1)}, u32[]{:S(2)}) copy-start(bf16[1,512,2048]{2,1,0:T(8,128)(2,1)} %param.35) | copy-start | bytes 6291460
  7.2 103.2 %copy-start.3 = (bf16[16,2048]{1,0:T(8,128)(2,1)S(1)}, bf16[16,2048]{1,0:T(8,128)(2,1)}, u32[]{:S(2)}) copy-start(bf16[16,2048]{1,0:T(8,128)(2,1)} %param.20) | copy-start | bytes 196612
  7.2 98.1 %all-gather.4.cloned.1.call-start = ((), (), s32[]{:S(2)}) async-start(), calls=%async_computation.5 | async-start | bytes 12779520 | tf_op jit(solution)/shard_map/all_gather | solution.py:13
  9.0 164.4 %all-gather.6.cloned.1.call-start = ((), (), s32[]{:S(2)}) async-start(), calls=%async_computation.6 | async-start | bytes 3194880 | tf_op jit(solution)/shard_map/all_gather | solution.py:148
  9.7 244.0 %all-gather.8.cloned.1.call-start = ((), (), s32[]{:S(2)}) async-start(), calls=%async_computation.7 | async-start | bytes 4259840 | tf_op jit(solution)/shard_map/all_gather | solution.py:188
  117.6 2.7 copy-start.2
  125.7 58.8 %copy-start.6 = (s32[16,4]{0,1:T(4,128)S(1)}, s32[16,4]{0,1:T(4,128)}, u32[]{:S(2)}) copy-start(s32[16,4]{0,1:T(4,128)} %param.31) | copy-start | bytes 772
  125.8 59.5 %copy-start.8 = (bf16[16,4]{0,1:T(4,128)(2,1)S(1)}, bf16[16,4]{0,1:T(4,128)(2,1)}, u32[]{:S(2)}) copy-start(bf16[16,4]{0,1:T(4,128)(2,1)} %param.32) | copy-start | bytes 388
  173.4 20.4 %copy-start.7 = (bf16[2048]{0:T(1024)(128)(2,1)S(1)}, bf16[2048]{0:T(1024)(128)(2,1)}, u32[]{:S(2)}) copy-start(bf16[2048]{0:T(1024)(128)(2,1)} %param.39) | copy-start | bytes 12292
  187.7 19.0 %all-to-all-start.2 = ((bf16[64,2,2048]{2,1,0:T(2,128)(2,1)}), bf16[64,2,2048]{2,1,0:T(2,128)(2,1)S(1)}, u32[]{:S(2)}, u32[]{:S(2)}) async-start(bf16[64,2,2048]{2,1,0:T(2,128)(2,1)} %reshape.197), calls=%async_computation.2 | async-start | bytes 1048576 | tf_op jit(solution)/shard_map/all_to_all | solution.py:168
  212.6 52.8 %all-to-all-start.3 = ((bf16[64,2,2048]{2,1,0:T(2,128)(2,1)}), bf16[64,2,2048]{2,1,0:T(2,128)(2,1)S(1)}, u32[]{:S(2)}, u32[]{:S(2)}) async-start(bf16[64,2,2048]{2,1,0:T(2,128)(2,1)} %copy.47), calls=%async_computation.3 | async-start | bytes 1048576 | tf_op jit(solution)/shard_map/all_to_all | solution.py:177
  217.4 41.2 %copy-start.4 = (bf16[32,2048]{1,0:T(8,128)(2,1)S(1)}, bf16[32,2048]{1,0:T(8,128)(2,1)}, u32[]{:S(2)}) copy-start(bf16[32,2048]{1,0:T(8,128)(2,1)} %param.38) | copy-start | bytes 393220
  217.4 41.2 %copy-start.5 = (bf16[2048,32]{0,1:T(8,128)(2,1)S(1)}, bf16[2048,32]{0,1:T(8,128)(2,1)}, u32[]{:S(2)}) copy-start(bf16[2048,32]{0,1:T(8,128)(2,1)} %param.37) | copy-start | bytes 393220
  253.8 3.7 %copy-start.1 = (bf16[1024,2048]{1,0:T(8,128)(2,1)S(1)}, bf16[1024,2048]{1,0:T(8,128)(2,1)}, u32[]{:S(2)}) copy-start(bf16[1024,2048]{1,0:T(8,128)(2,1)} %all-gather.8.cloned.1.call-done) | copy-start | bytes 12582916
  265.4 57.4 %all-to-all-start.1 = ((bf16[64,16,2048]{2,1,0:T(8,128)(2,1)}), bf16[64,16,2048]{2,1,0:T(8,128)(2,1)}, u32[]{:S(2)}, u32[]{:S(2)}) async-start(bf16[64,16,2048]{2,1,0:T(8,128)(2,1)} %bitcast.86), calls=%async_computation.1 | async-start | bytes 8388608 | tf_op jit(solution)/shard_map/all_to_all | solution.py:37
Sparse Core Ops, SparseCore 0:
  11.3 93.9 all-gather.3
  108.1 65.2 all-gather.5
  184.6 69.0 all-gather.7
where the time goes:
time: 341 us
  waiting for transfers between devices  239 us (70%)
  matrix products  34.9 us (10%)
  starting transfers between devices  17.9 us (5%)
  other arithmetic  15.6 us (5%)
  between operations  14.1 us (4%)
  blocking collectives  13.2 us (4%)
  local copies, waits for them, and re-layouts  6 us (2%)
    all_gather x1, waiting for transfers between devices, in_one_piece(): out, at, done = (lax.all_gather(both, axis, axis=dim, tiled=True), 0, [])  91.6 us
    all_to_all x1, waiting for transfers between devices, summed_on_arrival(): tiles = lax.all_to_all(split_up(array, dim, size), axis, 0, 0, tiled=True)  50.4 us
    all_gather x1, waiting for transfers between devices, on_device(): lax.all_gather(w_out, 'ep', axis=1, tiled=True)  47.2 us
    all_gather x1, waiting for transfers between devices, on_device(): segment = lax.all_gather(normed_ffn, 'ep', axis=0, tiled=True)  36.3 us
    all_to_all x2, blocking collectives, sent_to_all(): return lax.all_to_all(copies, axis, split_axis=0, concat_axis=0, tiled=True)  13.2 us
    all_to_all x1, waiting for transfers between devices, on_device(): lax.all_to_all(outgoing, 'ep', split_axis=0, concat_axis=0, tiled=True)  12.9 us
    dot_general x3, matrix products, on_device(): jnp.dot(normed, weight_rows, preferred_element_type=jnp.float32)  7.44 us
  transfers between devices with their start and end apart: 6, of which 5 were waited for; matrix products, arithmetic and copies ran while one was open for 13% of the time, Pallas kernels for 0%

commit v1 on v0

--- a/solution.py
+++ b/solution.py
@@ -145,7 +145,9 @@
     )
     partial_rows = jnp.dot(
         retained,
-        lax.all_gather(w_out, "ep", axis=1, tiled=True),
+        jnp.concatenate(
+            lax.all_to_all(jnp.stack(lax.axis_size("ep") * [w_out], 0), "ep", 0, 0), axis=1
+        ),
         preferred_element_type=jnp.float32,
     )
     rounded = lax.optimization_barrier(partial_rows.astype(jnp.bfloat16)).astype(jnp.float32)

time: 341 us -> 325 us (0.953)
  waiting for transfers between devices: 239 us -> 210 us
  starting transfers between devices: 17.9 us -> 32.2 us
  other arithmetic: 15.6 us -> 12 us
    all_gather x1 -> x0, waiting for transfers between devices: 47.2 us -> none  [on_device(): lax.all_gather(w_out, 'ep', axis=1, tiled=True)]
    all_gather x1, waiting for transfers between devices: 91.6 us -> 110 us  [in_one_piece(): out, at, done = (lax.all_gather(both, axis, axis=dim, tiled=True), 0, [])]
    all_to_all x0 -> x1, starting transfers between devices: none -> 12.2 us  [on_device(): lax.all_to_all(jnp.stack(lax.axis_size('ep') * [w_out], 0), 'ep', 0, 0)]
  transfers between devices with their start and end apart: 6 -> 6, of which waited for: 5 -> 4; matrix products, arithmetic and copies ran while one was open for 13% -> 13% of each run, Pallas kernels for 0% -> 0%
where the time goes in v1:
time: 325 us; the launch traced here: 324 us
  waiting for transfers between devices  210 us (65%)
  matrix products  34.8 us (11%)
  starting transfers between devices  32.2 us (10%)
  between operations  14.5 us (4%)
  other arithmetic  12 us (4%)
  blocking collectives  11.8 us (4%)
  local copies, waits for them, and re-layouts  8.9 us (3%)
    all_gather x1, waiting for transfers between devices, in_one_piece(): out, at, done = (lax.all_gather(both, axis, axis=dim, tiled=True), 0, [])  110 us
    all_to_all x1, waiting for transfers between devices, summed_on_arrival(): tiles = lax.all_to_all(split_up(array, dim, size), axis, 0, 0, tiled=True)  50.4 us
    all_gather x1, waiting for transfers between devices, on_device(): segment = lax.all_gather(normed_ffn, 'ep', axis=0, tiled=True)  37.1 us
    all_to_all x1, waiting for transfers between devices, on_device(): lax.all_to_all(outgoing, 'ep', split_axis=0, concat_axis=0, tiled=True)  12.7 us
    all_to_all x1, starting transfers between devices, on_device(): lax.all_to_all(jnp.stack(lax.axis_size('ep') * [w_out], 0), 'ep', 0, 0)  12.2 us
    all_to_all x2, blocking collectives, sent_to_all(): return lax.all_to_all(copies, axis, split_axis=0, concat_axis=0, tiled=True)  11.8 us
    all_to_all x1, starting transfers between devices, on_device(): lax.all_to_all(outgoing, 'ep', split_axis=0, concat_axis=0, tiled=True)  8.5 us
    dot_general x3, matrix products, on_device(): jnp.dot(normed, weight_rows, preferred_element_type=jnp.float32)  7.36 us
  transfers between devices with their start and end apart: 6, of which 4 were waited for; matrix products, arithmetic and copies ran while one was open for 13% of the time, Pallas kernels for 0%

profile of v1, /device:TPU:1, one launch (start us, length us, event | category | flops | bytes accessed | tf_op | source)
XLA Modules:
  0.0 324.0 jit_solution(8663117152856904478)
XLA Ops:
  7.2 1.7 pad_maximum_fusion
  9.0 2.9 stack.2
  11.9 12.2 %all-to-all-start = ((bf16[64,768,32]{1,2,0:T(8,128)(2,1)}), bf16[64,768,32]{1,2,0:T(8,128)(2,1)}, u32[]{:S(2)}, u32[]{:S(2)}) async-start(bf16[64,768,32]{1,2,0:T(8,128)(2,1)} %stack.2), calls=%async_computation | async-start | bytes 6291456 | tf_op jit(solution)/shard_map/all_to_all | solution.py:149
  24.2 0.1 dynamic-slice_exponential_fusion
  24.3 0.1 fusion.64
  24.5 0.1 multiply_cosine_fusion
  24.6 109.6 %all-gather.3.cloned.1.call-done = bf16[2048,3072]{1,0:T(8,128)(2,1)} async-done(((bf16[32,3072]{1,0:T(8,128)(2,1)}), bf16[2048,3072]{1,0:T(8,128)(2,1)}) %all-gather.3.cloned.1.call-update) | async-done | bytes 12582928 | tf_op jit(solution)/shard_map/all_gather | solution.py:13
  134.2 2.4 fusion.45
  136.7 2.4 fusion.39
  139.2 2.5 fusion.33
  141.7 0.1 multiply_subtract_fusion.1
  141.8 0.1 maximum_bitcast_fusion
  141.9 0.1 maximum_multiply_fusion
  141.9 4.5 %multiply_add_fusion = f32[16,6,128,128]{3,2,1,0:T(8,128)S(1)} fusion(f32[16,6,128,128]{3,2,1,0:T(8,128)} %param.22, f32[16,6,128]{2,1,0:T(8,128)S(1)} %reshape.217, f32[16,6,128]{2,1,0:T(8,128)S(1)} %maximum_multiply_fusion, f32[6]{0:T(128)S(1)} %dynamic-slice_exponential_fusion), kind=kLoop, calls=%fused_computation.2 | loop fusion | flops 4718592 | bytes 12681240 | tf_op jit(solution)/shard_map/add | solution.py:80
  146.4 2.7 copy-done.2
  149.1 5.5 %fusion.84 = f32[16,6,1,128]{3,2,1,0:T(1,128)S(1)} fusion(f32[16,6,128,128]{3,2,1,0:T(8,128)S(1)} %multiply_add_fusion, f32[16,6,128,1]{2,1,0,3:T(8,128)S(1)} %maximum_bitcast_fusion), kind=kOutput, calls=%fused_computation.80 | convolution fusion | flops 18874368 | bytes 6389760 | tf_op jit(solution)/shard_map/shd,shdv->shv/dot_general | solution.py:83
  154.6 0.1 bitcast_reduce_fusion
  154.7 0.2 fusion.80
  154.9 0.1 fusion.81
  155.0 4.5 %convolution_convert_fusion.2 = bf16[16,2048]{1,0:T(8,128)(2,1)S(1)} fusion(bf16[768,2048]{0,1:T(8,128)(2,1)} %bitcast.4, f32[2,8,6,128]{3,2,1,0:T(8,128)S(1)} %bitcast.90, bf16[2048,3072]{1,0:T(8,128)(2,1)} %all-gather.3.cloned.1.call-done, bf16[16,2048]{1,0:T(8,128)(2,1)S(1)} %copy-done.3, f32[2048]{0:T(1024)S(1)} %convert_element_type.100, ...), kind=kOutput, calls=%fused_computation.15 | convolution fusion | flops 100925440 | bytes 6479936 | tf_op jit(solution)/shard_map/dot_general | solution.py:146
  159.5 4.3 %all_to_all.30 = bf16[2,16,2048]{2,1,0:T(8,128)(2,1)S(1)} all-to-all(bf16[2,16,2048]{2,1,0:T(8,128)(2,1)S(1)} %broadcast_in_dim.4), channel_id=1, replica_groups=mesh['ep'=64,'tp'=2] {'tp'}, dimensions={0} | all-to-all | bytes 262144 | tf_op jit(solution)/shard_map/all_to_all | solution.py:22
  163.9 0.1 fusion.68
  164.0 0.7 fusion.70
  164.8 0.1 copy.44
  164.9 0.1 eq.31
  165.0 0.1 reduce_window_sum.11
  165.1 0.2 select_reduce_fusion.1
  165.4 0.1 copy.45
  165.5 0.1 convert_reduce_fusion.2
  165.6 1.2 convolution_convert_fusion.1
  166.8 1.1 reshape.207
  167.9 8.5 %all-to-all-start.3 = ((bf16[64,2,2048]{2,1,0:T(2,128)(2,1)}), bf16[64,2,2048]{2,1,0:T(2,128)(2,1)S(1)}, u32[]{:S(2)}, u32[]{:S(2)}) async-start(bf16[64,2,2048]{2,1,0:T(2,128)(2,1)} %reshape.207), calls=%async_computation.3 | async-start | bytes 1048576 | tf_op jit(solution)/shard_map/all_to_all | solution.py:170
  176.5 12.7 %all-to-all-done.3 = bf16[64,2,2048]{2,1,0:T(2,128)(2,1)S(1)} async-done(((bf16[64,2,2048]{2,1,0:T(2,128)(2,1)}), bf16[64,2,2048]{2,1,0:T(2,128)(2,1)S(1)}, u32[]{:S(2)}, u32[]{:S(2)}) %all-to-all-start.3) | async-done | bytes 524320 | tf_op jit(solution)/shard_map/all_to_all | solution.py:170
  189.1 2.0 fusion.14
  191.2 2.5 convolution_convert_fusion
  193.7 1.4 copy.48
  195.1 4.6 %all-to-all-start.4 = ((bf16[64,2,2048]{2,1,0:T(2,128)(2,1)}), bf16[64,2,2048]{2,1,0:T(2,128)(2,1)S(1)}, u32[]{:S(2)}, u32[]{:S(2)}) async-start(bf16[64,2,2048]{2,1,0:T(2,128)(2,1)} %copy.48), calls=%async_computation.4 | async-start | bytes 1048576 | tf_op jit(solution)/shard_map/all_to_all | solution.py:179
  199.7 37.1 %all-gather.5.cloned.1.call-done = bf16[1024,2048]{1,0:T(8,128)(2,1)} async-done(((bf16[16,2048]{1,0:T(8,128)(2,1)}), bf16[1024,2048]{1,0:T(8,128)(2,1)}) %all-gather.5.cloned.1.call-update) | async-done | bytes 4194320 | tf_op jit(solution)/shard_map/all_gather | solution.py:190
  236.8 3.5 %fusion.102 = f32[1,1024]{1,0:T(1,128)S(1)} fusion(bf16[1024,2048]{1,0:T(8,128)(2,1)} %all-gather.5.cloned.1.call-done, bf16[2048,1]{0,1:T(2,128)(2,1)S(1)} %reshape.221), kind=kOutput, calls=%fused_computation.108 | convolution fusion | flops 4194304 | bytes 4202496 | tf_op jit(solution)/shard_map/dot_general | solution.py:195
  240.3 1.3 fusion.101
  241.7 6.7 %multiply_convert_fusion = bf16[1024,2048]{1,0:T(8,128)(2,1)} fusion(bf16[32,2048]{1,0:T(8,128)(2,1)S(1)} %copy-done.4, f32[1024]{0:T(1024)S(1)} %add_divide_fusion, bf16[1024,2048]{1,0:T(8,128)(2,1)} %all-gather.5.cloned.1.call-done, bf16[2048,32]{0,1:T(8,128)(2,1)S(1)} %copy-done.5, f32[1024,32]{0,1:T(8,128)S(1)} %fusion.101), kind=kOutput, calls=%fused_computation.1 | convolution fusion | flops 272826368 | bytes 8785920 | tf_op jit(solution)/shard_map/dot_general | solution.py:197
  248.4 6.8 %all-to-all-start.2 = ((bf16[64,16,2048]{2,1,0:T(8,128)(2,1)}), bf16[64,16,2048]{2,1,0:T(8,128)(2,1)}, u32[]{:S(2)}, u32[]{:S(2)}) async-start(bf16[64,16,2048]{2,1,0:T(8,128)(2,1)} %bitcast.89), calls=%async_computation.2 | async-start | bytes 8388608 | tf_op jit(solution)/shard_map/all_to_all | solution.py:37
  255.2 0.2 reshape.212
  255.4 50.4 %all-to-all-done.2 = bf16[64,16,2048]{2,1,0:T(8,128)(2,1)} async-done(((bf16[64,16,2048]{2,1,0:T(8,128)(2,1)}), bf16[64,16,2048]{2,1,0:T(8,128)(2,1)}, u32[]{:S(2)}, u32[]{:S(2)}) %all-to-all-start.2) | async-done | bytes 4194336 | tf_op jit(solution)/shard_map/all_to_all | solution.py:37
  305.8 2.9 convert_reduce_fusion
  308.7 0.3 fusion.8
  309.0 7.5 %all_to_all.31 = bf16[2,16,2048]{2,1,0:T(8,128)(2,1)S(1)} all-to-all(bf16[2,16,2048]{2,1,0:T(8,128)(2,1)S(1)} %broadcast_in_dim.5), channel_id=1, replica_groups=mesh['ep'=64,'tp'=2] {'tp'}, dimensions={0} | all-to-all | bytes 262144 | tf_op jit(solution)/shard_map/all_to_all | solution.py:22
  316.5 0.7 fusion.71
  (57 shorter events, 0.6 us)
Async XLA Ops:
  7.2 184.0 %copy-start = (bf16[1,512,2048]{2,1,0:T(8,128)(2,1)S(1)}, bf16[1,512,2048]{2,1,0:T(8,128)(2,1)}, u32[]{:S(2)}) copy-start(bf16[1,512,2048]{2,1,0:T(8,128)(2,1)} %param.35) | copy-start | bytes 6291460
  7.2 127.0 %all-gather.3.cloned.1.call-start = ((), (), s32[]{:S(2)}) async-start(), calls=%async_computation.6 | async-start | bytes 12779520 | tf_op jit(solution)/shard_map/all_gather | solution.py:13
  9.0 15.2 %copy-start.13 = (s32[16]{0:T(128)S(1)}, s32[16]{0:T(128)}, u32[]{:S(2)}) copy-start(s32[16]{0:T(128)} %param.21) | copy-start | bytes 196
  9.0 15.2 %copy-start.8 = (bf16[2048]{0:T(1024)(128)(2,1)S(1)}, bf16[2048]{0:T(1024)(128)(2,1)}, u32[]{:S(2)}) copy-start(bf16[2048]{0:T(1024)(128)(2,1)} %param.23) | copy-start | bytes 12292
  9.0 15.2 %copy-start.9 = (bf16[2048]{0:T(1024)(128)(2,1)S(1)}, bf16[2048]{0:T(1024)(128)(2,1)}, u32[]{:S(2)}) copy-start(bf16[2048]{0:T(1024)(128)(2,1)} %param.30) | copy-start | bytes 12292
  9.0 15.3 %copy-start.3 = (bf16[16,2048]{1,0:T(8,128)(2,1)S(1)}, bf16[16,2048]{1,0:T(8,128)(2,1)}, u32[]{:S(2)}) copy-start(bf16[16,2048]{1,0:T(8,128)(2,1)} %param.20) | copy-start | bytes 196612
  9.0 15.5 %copy-start.11 = (bf16[768]{0:T(1024)(128)(2,1)S(1)}, bf16[768]{0:T(1024)(128)(2,1)}, u32[]{:S(2)}) copy-start(bf16[768]{0:T(1024)(128)(2,1)} %param.28) | copy-start | bytes 4612
  11.9 143.1 %all-to-all-start = ((bf16[64,768,32]{1,2,0:T(8,128)(2,1)}), bf16[64,768,32]{1,2,0:T(8,128)(2,1)}, u32[]{:S(2)}, u32[]{:S(2)}) async-start(bf16[64,768,32]{1,2,0:T(8,128)(2,1)} %stack.2), calls=%async_computation | async-start | bytes 6291456 | tf_op jit(solution)/shard_map/all_to_all | solution.py:149
  24.1 212.7 %all-gather.5.cloned.1.call-start = ((), (), s32[]{:S(2)}) async-start(), calls=%async_computation.7 | async-start | bytes 4259840 | tf_op jit(solution)/shard_map/all_gather | solution.py:190
  146.4 2.7 copy-start.2
  154.6 10.2 %copy-start.7 = (s32[16,4]{0,1:T(4,128)S(1)}, s32[16,4]{0,1:T(4,128)}, u32[]{:S(2)}) copy-start(s32[16,4]{0,1:T(4,128)} %param.31) | copy-start | bytes 772
  154.6 10.9 %copy-start.12 = (bf16[16,4]{0,1:T(4,128)(2,1)S(1)}, bf16[16,4]{0,1:T(4,128)(2,1)}, u32[]{:S(2)}) copy-start(bf16[16,4]{0,1:T(4,128)(2,1)} %param.32) | copy-start | bytes 388
  155.0 21.5 %copy-start.10 = (bf16[2048]{0:T(1024)(128)(2,1)S(1)}, bf16[2048]{0:T(1024)(128)(2,1)}, u32[]{:S(2)}) copy-start(bf16[2048]{0:T(1024)(128)(2,1)} %param.39) | copy-start | bytes 12292
  167.9 21.2 %all-to-all-start.3 = ((bf16[64,2,2048]{2,1,0:T(2,128)(2,1)}), bf16[64,2,2048]{2,1,0:T(2,128)(2,1)S(1)}, u32[]{:S(2)}, u32[]{:S(2)}) async-start(bf16[64,2,2048]{2,1,0:T(2,128)(2,1)} %reshape.207), calls=%async_computation.3 | async-start | bytes 1048576 | tf_op jit(solution)/shard_map/all_to_all | solution.py:170
  193.7 46.7 %copy-start.6 = (bf16[2048,32]{0,1:T(8,128)(2,1)S(1)}, bf16[2048,32]{0,1:T(8,128)(2,1)}, u32[]{:S(2)}) copy-start(bf16[2048,32]{0,1:T(8,128)(2,1)} %param.36) | copy-start | bytes 393220
  195.1 53.4 %all-to-all-start.4 = ((bf16[64,2,2048]{2,1,0:T(2,128)(2,1)}), bf16[64,2,2048]{2,1,0:T(2,128)(2,1)S(1)}, u32[]{:S(2)}, u32[]{:S(2)}) async-start(bf16[64,2,2048]{2,1,0:T(2,128)(2,1)} %copy.48), calls=%async_computation.4 | async-start | bytes 1048576 | tf_op jit(solution)/shard_map/all_to_all | solution.py:179
  199.7 42.0 %copy-start.4 = (bf16[32,2048]{1,0:T(8,128)(2,1)S(1)}, bf16[32,2048]{1,0:T(8,128)(2,1)}, u32[]{:S(2)}) copy-start(bf16[32,2048]{1,0:T(8,128)(2,1)} %param.38) | copy-start | bytes 393220
  199.7 42.0 %copy-start.5 = (bf16[2048,32]{0,1:T(8,128)(2,1)S(1)}, bf16[2048,32]{0,1:T(8,128)(2,1)}, u32[]{:S(2)}) copy-start(bf16[2048,32]{0,1:T(8,128)(2,1)} %param.37) | copy-start | bytes 393220
  236.8 3.5 %copy-start.1 = (bf16[1024,2048]{1,0:T(8,128)(2,1)S(1)}, bf16[1024,2048]{1,0:T(8,128)(2,1)}, u32[]{:S(2)}) copy-start(bf16[1024,2048]{1,0:T(8,128)(2,1)} %all-gather.5.cloned.1.call-done) | copy-start | bytes 12582916
  248.4 57.4 %all-to-all-start.2 = ((bf16[64,16,2048]{2,1,0:T(8,128)(2,1)}), bf16[64,16,2048]{2,1,0:T(8,128)(2,1)}, u32[]{:S(2)}, u32[]{:S(2)}) async-start(bf16[64,16,2048]{2,1,0:T(8,128)(2,1)} %bitcast.89), calls=%async_computation.2 | async-start | bytes 8388608 | tf_op jit(solution)/shard_map/all_to_all | solution.py:37
Sparse Core Ops, SparseCore 0:
  11.3 122.8 all-gather.2
  164.9 71.8 all-gather.4
